TPU v7x, 256 devices: a whole 4x4x8 slice. The times are simulated.
256 devices in a mesh: ep: 16 (over y, x), tp: 16 (over z, core).
Axes of the slice: x: 4, y: 4, z: 8, core: 2. Of those that a mesh axis runs over, the one named last changes fastest.
Arguments:
- tokens: bfloat16 [1024, 4096], P('ep'), may hold values from -6 to 6
- norm_gain: float32 [4096], replicated, may hold values from 0.1 to 1.9
- ffn_gain: float32 [4096], replicated, may hold values from 0.1 to 1.9
- w_in: bfloat16 [4096, 2048], P(None, 'tp'), may hold values from -0.09375 to 0.09375
- decay_rate: float32 [8192], P('tp'), may hold values from 0.02 to 2
- frequency: float32 [8192], P('tp'), may hold values from -3.140625 to 3.140625
- log_step: float32 [128], P('tp'), may hold values from -2.3 to 0
- input_real: float32 [16, 8192], P(None, 'tp'), may hold values from -1 to 1
- input_imag: float32 [16, 8192], P(None, 'tp'), may hold values from -1 to 1
- readout_real: float32 [16, 8192], P(None, 'tp'), may hold values from -0.5 to 0.5
- readout_imag: float32 [16, 8192], P(None, 'tp'), may hold values from -0.5 to 0.5
- skip_gain: float32 [2048], P('tp'), may hold values from -4 to 4
- state_real: float32 [1024, 8192], P('ep', 'tp'), may hold values from -6 to 6
- state_imag: float32 [1024, 8192], P('ep', 'tp'), may hold values from -6 to 6
- w_out: bfloat16 [2048, 4096], P('tp'), may hold values from -0.125 to 0.125
- shared_gate: bfloat16 [4096, 1024], P(None, 'tp'), may hold values from -0.09375 to 0.09375
- shared_up: bfloat16 [4096, 1024], P(None, 'tp'), may hold values from -0.09375 to 0.09375
- shared_down: bfloat16 [1024, 4096], P('tp'), may hold values from -0.1875 to 0.1875
- expert_gate: bfloat16 [64, 4096, 1024], P('ep', 'tp'), may hold values from -0.09375 to 0.09375
- expert_up: bfloat16 [64, 4096, 1024], P('ep', 'tp'), may hold values from -0.09375 to 0.09375
- expert_down: bfloat16 [64, 1024, 4096], P('ep', None, 'tp'), may hold values from -0.1875 to 0.1875
- routing: int32 [1024, 4], P('ep'), may hold values from 0 to 63, all different within a row; in each aligned block of 64 rows (0 to 63, 64 to 127, ...) at most 8 rows name the same one
- route_weight: float32 [1024, 4], P('ep'), may hold values from 0.1 to 1
Outputs:
- mixed: bfloat16 [1024, 4096], P('ep', 'tp')
- new_state_real: float32 [1024, 8192], P('ep', 'tp')
- new_state_imag: float32 [1024, 8192], P('ep', 'tp')
Inputs may be any that keep to these rules, and one draw needn't show every extreme that they name: `routing`: each row names 4 different experts. In the rows of one index of ep (aligned blocks of 64 rows) no expert is named more than 8 times, and in every draw some expert is named exactly 8 times in some block.
All inputs are finite; a program needn't handle non-finite values.
Results may differ from a plain program's by a relative error of at most 0.02.
Values may be sent and summed in bfloat16 or wider, within the bound.
A program may use at most 64 MiB of HBM per device.

v0:
```python
import jax
import jax.numpy as jnp
from jax import lax
from jax.sharding import PartitionSpec as P

EPS = 1e-06
ROUTED_SCALE = 2.5
HIGH = lax.Precision.HIGHEST


def split_up(x, dim, peers):
    dims = x.shape
    parts = x.reshape(*dims[:dim], peers, dims[dim] // peers, *dims[dim + 1 :])
    return jnp.moveaxis(parts, dim, 0)


def sent_and_summed(x, axis, dim):
    parts = split_up(x, dim, lax.axis_size(axis))
    arrived = lax.all_to_all(parts, axis, split_axis=0, concat_axis=0, tiled=True)
    return arrived.astype(jnp.float32).sum(axis=0)


def sent_to_all(x, axis):
    copies = jnp.broadcast_to(x, (lax.axis_size(axis), *x.shape))
    return lax.all_to_all(copies, axis, split_axis=0, concat_axis=0, tiled=True)


def over_copies(x, axis):
    everything = sent_to_all(x, axis)
    return jnp.sum(everything, axis=0)


def joined_along(parts, dim):
    parts = jnp.moveaxis(parts, 0, dim)
    dims = parts.shape
    return parts.reshape(*dims[:dim], dims[dim] * dims[dim + 1], *dims[dim + 2 :])


def gathered_copies(x, axis, dim):
    return joined_along(sent_to_all(x, axis), dim)


def in_one(arrays, axis):
    line, at, finished = (jnp.concatenate([a.reshape(-1) for a in arrays]), 0, [])
    total = lax.psum(line, axis)
    for a in arrays:
        finished.append(total[at : at + a.size].reshape(a.shape))
        at += a.size
    return tuple(finished)


def rms_scale(values_in, gains):
    values = values_in.astype(jnp.float32)
    factor = lax.rsqrt(jnp.mean(values * values, axis=-1, keepdims=True) + EPS)
    return (values * factor * gains).astype(jnp.bfloat16)


def state_update(
    normed,
    w_in,
    decay_rate,
    frequency,
    log_step,
    input_real,
    input_imag,
    readout_real,
    readout_imag,
    skip_gain,
    state_real,
    state_imag,
):
    seq_count = normed.shape[0]
    groups = log_step.shape[0]
    chan_count = skip_gain.shape[0] // groups
    state_width = decay_rate.shape[0] // groups
    drive_rows = jnp.dot(normed, w_in, preferred_element_type=jnp.float32).astype(jnp.bfloat16)
    drive_f = drive_rows.astype(jnp.float32).reshape(seq_count, groups, chan_count)
    decays = decay_rate.reshape(groups, state_width)
    omegas = frequency.reshape(groups, state_width)
    step_size = jnp.exp(log_step)[:, None]
    pole_mag = jnp.exp(-decays * step_size)
    pole_angle = omegas * step_size
    pole_re = pole_mag * jnp.cos(pole_angle)
    pole_im = pole_mag * jnp.sin(pole_angle)
    pole_norm = decays * decays + omegas * omegas
    diff_re = pole_re - 1.0
    lift_re = (-decays * diff_re + omegas * pole_im) / pole_norm
    lift_im = (-decays * pole_im - omegas * diff_re) / pole_norm
    in_re = input_real.reshape(chan_count, groups, state_width)
    in_im = input_imag.reshape(chan_count, groups, state_width)
    push_re = jnp.einsum("sgh,hgp->sgp", drive_f, in_re, precision=HIGH)
    push_im = jnp.einsum("sgh,hgp->sgp", drive_f, in_im, precision=HIGH)
    old_re = state_real.reshape(seq_count, groups, state_width)
    old_im = state_imag.reshape(seq_count, groups, state_width)
    new_re = pole_re * old_re - pole_im * old_im + lift_re * push_re - lift_im * push_im
    new_im = pole_re * old_im + pole_im * old_re + lift_re * push_im + lift_im * push_re
    out_re = readout_real.reshape(chan_count, groups, state_width)
    out_im = readout_imag.reshape(chan_count, groups, state_width)
    read_rows = jnp.einsum("sgp,hgp->sgh", new_re, out_re, precision=HIGH) - jnp.einsum(
        "sgp,hgp->sgh", new_im, out_im, precision=HIGH
    )
    read_rows = read_rows + skip_gain.reshape(groups, chan_count) * drive_f
    activated = jax.nn.gelu(read_rows).reshape(seq_count, groups * chan_count).astype(jnp.bfloat16)
    return (
        activated,
        new_re.reshape(seq_count, groups * state_width),
        new_im.reshape(seq_count, groups * state_width),
    )


def local(
    tokens,
    norm_gain,
    ffn_gain,
    w_in,
    decay_rate,
    frequency,
    log_step,
    input_real,
    input_imag,
    readout_real,
    readout_imag,
    skip_gain,
    state_real,
    state_imag,
    w_out,
    shared_gate,
    shared_up,
    shared_down,
    expert_gate,
    expert_up,
    expert_down,
    routing,
    route_weight,
):
    seq_count, model_width = tokens.shape
    tp_count = lax.axis_size("tp")
    ep_count = lax.axis_size("ep")
    slice_width = model_width // tp_count
    offset = lax.axis_index("tp") * slice_width
    normed = rms_scale(tokens, norm_gain)
    activated, new_real, new_imag = state_update(
        normed,
        w_in,
        decay_rate,
        frequency,
        log_step,
        input_real,
        input_imag,
        readout_real,
        readout_imag,
        skip_gain,
        state_real,
        state_imag,
    )
    mixer_terms = jnp.dot(activated, w_out, preferred_element_type=jnp.float32)
    mixer_own = sent_and_summed(mixer_terms.astype(jnp.bfloat16), "tp", 1)
    own_tokens = lax.dynamic_slice_in_dim(tokens, offset, slice_width, 1)
    resid_own = (own_tokens.astype(jnp.float32) + mixer_own).astype(jnp.bfloat16)
    resid_f = resid_own.astype(jnp.float32)
    square_sum = over_copies(jnp.sum(resid_f * resid_f, axis=1, keepdims=True), "tp")
    factor = lax.rsqrt(square_sum / model_width + EPS)
    gain_own = lax.dynamic_slice_in_dim(ffn_gain, offset, slice_width, 0)
    rows_own = (resid_f * factor * gain_own).astype(jnp.bfloat16)
    ffn_rows = gathered_copies(rows_own, "tp", 1)
    expert_dev = expert_gate.shape[0]
    expert_count = expert_dev * ep_count
    top_count = routing.shape[1]
    capacity = 2 * seq_count * top_count // expert_count
    slot_count = expert_count * capacity
    flat_ids = routing.reshape(-1)
    one_hot = (flat_ids[:, None] == jnp.arange(expert_count, dtype=jnp.int32)[None, :]).astype(
        jnp.int32
    )
    earlier = jnp.cumsum(one_hot, axis=0) - one_hot
    slot_rank = jnp.sum(earlier * one_hot, axis=1)
    target = flat_ids * capacity + slot_rank
    slot_ids = jnp.arange(slot_count, dtype=jnp.int32)
    placed = (target[None, :] == slot_ids[:, None]).reshape(slot_count, seq_count, top_count)
    dispatch_map = jnp.sum(placed.astype(jnp.float32), axis=2).astype(jnp.bfloat16)
    outgoing = jnp.dot(dispatch_map, rows_own, preferred_element_type=jnp.float32).astype(
        jnp.bfloat16
    )
    outgoing = outgoing.reshape(ep_count, expert_dev * capacity, slice_width)
    incoming = lax.all_to_all(outgoing, "ep", split_axis=0, concat_axis=0, tiled=True)
    arrived = incoming.reshape(ep_count, expert_dev, capacity, slice_width)
    gate_part = jnp.einsum(
        "secd,edf->secf", arrived, expert_gate, preferred_element_type=jnp.float32
    )
    up_part = jnp.einsum("secd,edf->secf", arrived, expert_up, preferred_element_type=jnp.float32)
    gate_full, up_full = tuple(
        (
            part.astype(jnp.float32)
            for part in in_one((gate_part.astype(jnp.bfloat16), up_part.astype(jnp.bfloat16)), "tp")
        )
    )
    inner_rows = (jax.nn.silu(gate_full) * up_full).astype(jnp.bfloat16)
    expert_terms = jnp.einsum(
        "secf,efd->secd", inner_rows, expert_down, preferred_element_type=jnp.float32
    )
    returned = lax.all_to_all(
        expert_terms.reshape(ep_count, expert_dev * capacity, slice_width).astype(jnp.bfloat16),
        "ep",
        split_axis=0,
        concat_axis=0,
        tiled=True,
    ).astype(jnp.float32)
    weights = route_weight / jnp.sum(route_weight, axis=1, keepdims=True) * ROUTED_SCALE
    chosen = target.reshape(seq_count, top_count)[:, :, None] == slot_ids[None, None, :]
    combine = jnp.sum(jnp.where(chosen, weights[:, :, None], 0.0), axis=1)
    routed = jnp.dot(combine, returned.reshape(slot_count, slice_width), precision=HIGH)
    shared_gate_rows = jnp.dot(ffn_rows, shared_gate, preferred_element_type=jnp.float32)
    shared_up_rows = jnp.dot(ffn_rows, shared_up, preferred_element_type=jnp.float32)
    shared_inner = (jax.nn.silu(shared_gate_rows) * shared_up_rows).astype(jnp.bfloat16)
    shared_terms = jnp.dot(shared_inner, shared_down, preferred_element_type=jnp.float32)
    shared_own = sent_and_summed(shared_terms.astype(jnp.bfloat16), "tp", 1)
    mixed = (resid_own.astype(jnp.float32) + shared_own + routed).astype(jnp.bfloat16)
    return (mixed, new_real, new_imag)


def solution(mesh):
    placed = (
        P("ep", None),
        P(),
        P(),
        P(None, "tp"),
        P("tp"),
        P("tp"),
        P("tp"),
        P(None, "tp"),
        P(None, "tp"),
        P(None, "tp"),
        P(None, "tp"),
        P("tp"),
        P("ep", "tp"),
        P("ep", "tp"),
        P("tp", None),
        P(None, "tp"),
        P(None, "tp"),
        P("tp", None),
        P("ep", "tp", None),
        P("ep", "tp", None),
        P("ep", None, "tp"),
        P("ep", None),
        P("ep", None),
    )
    return jax.shard_map(
        local,
        mesh=mesh,
        in_specs=placed,
        out_specs=(P("ep", "tp"), P("ep", "tp"), P("ep", "tp")),
        check_vma=False,
    )
```

profile of v0, /device:TPU:17, one launch (start us, length us, event | category | flops | bytes accessed | tf_op | source)
XLA Modules:
  0.0 234.6 jit_solution(10866147600172250460)
XLA Ops:
  7.2 0.8 exp.27
  8.1 1.2 fusion.28
  9.3 0.8 reshape.291
  10.1 0.7 mul.326
  10.8 0.7 fusion.67
  11.7 1.7 convolution_convert_fusion.3
  13.4 0.1 copy.114
  13.9 0.1 reshape.292
  14.0 0.1 reshape.293
  14.1 0.3 fusion.54
  14.4 0.1 cosine_multiply_fusion
  14.5 0.4 bitcast_add_fusion
  14.9 0.5 fusion.52
  15.5 0.6 fusion.44
  16.0 1.6 convolution_convert_fusion.1
  17.6 0.8 copy.170
  18.4 9.2 %all-to-all-start = ((bf16[16,64,256]{2,1,0:T(8,128)(2,1)}), bf16[16,64,256]{2,1,0:T(8,128)(2,1)S(1)}, u32[]{:S(2)}, u32[]{:S(2)}) async-start(bf16[16,64,256]{2,1,0:T(8,128)(2,1)} %bitcast.130), calls=%async_computation | async-start | bytes 1048576 | tf_op jit(solution)/shard_map/all_to_all | solution.py:19
  27.6 0.1 copy.124
  27.7 0.1 eq.56
  27.8 0.1 eq.52
  27.9 0.6 reduce-window.6
  28.5 0.2 slice_reduce_fusion
  28.8 0.1 fusion.50
  28.9 0.1 reduce_sum.89
  29.1 15.7 %all-to-all-done = bf16[16,64,256]{2,1,0:T(8,128)(2,1)S(1)} async-done(((bf16[16,64,256]{2,1,0:T(8,128)(2,1)}), bf16[16,64,256]{2,1,0:T(8,128)(2,1)S(1)}, u32[]{:S(2)}, u32[]{:S(2)}) %all-to-all-start) | async-done | bytes 524320 | tf_op jit(solution)/shard_map/all_to_all | solution.py:19
  44.9 0.9 fusion.45
  45.7 0.6 broadcast_in_dim.12
  46.4 3.4 %all-to-all-start.1 = ((f32[16,64,1]{1,2,0:T(1,128)}), f32[16,64,1]{1,2,0:T(1,128)S(1)}, u32[]{:S(2)}, u32[]{:S(2)}) async-start(f32[16,64,1]{1,2,0:T(1,128)} %broadcast_in_dim.12), calls=%async_computation.1 | async-start | bytes 16384 | tf_op jit(solution)/shard_map/all_to_all | solution.py:25
  49.7 0.1 convert_reduce_fusion.2
  49.9 0.8 dynamic_slice.7
  50.6 5.7 %all-to-all-done.1 = f32[16,64,1]{1,2,0:T(1,128)S(1)} async-done(((f32[16,64,1]{1,2,0:T(1,128)}), f32[16,64,1]{1,2,0:T(1,128)S(1)}, u32[]{:S(2)}, u32[]{:S(2)}) %all-to-all-start.1) | async-done | bytes 4128 | tf_op jit(solution)/shard_map/all_to_all | solution.py:25
  56.4 0.1 fusion.47
  56.5 0.2 convolution_convert_fusion.2
  56.7 12.1 %all_to_all.30 = bf16[16,32,256]{2,1,0:T(8,128)(2,1)S(1)} all-to-all(bf16[16,32,256]{2,1,0:T(8,128)(2,1)S(1)} %bitcast.134), channel_id=1, replica_groups=mesh['ep'=16,'tp'=16] {'ep'}, dimensions={0} | all-to-all | bytes 524288 | tf_op jit(solution)/shard_map/all_to_all | solution.py:185
  68.8 0.8 broadcast_in_dim.13
  69.6 5.3 %all-to-all-start.2 = ((bf16[16,64,256]{2,1,0:T(8,128)(2,1)}), bf16[16,64,256]{2,1,0:T(8,128)(2,1)S(1)}, u32[]{:S(2)}, u32[]{:S(2)}) async-start(bf16[16,64,256]{2,1,0:T(8,128)(2,1)} %broadcast_in_dim.13), calls=%async_computation.2 | async-start | bytes 1048576 | tf_op jit(solution)/shard_map/all_to_all | solution.py:25
  74.9 0.4 fusion.12
  75.4 0.1 copy.131
  75.5 0.3 copy.144
  75.8 1.2 copy-done.1
  77.0 0.4 fusion.15
  77.5 0.1 copy.129
  77.6 0.3 copy.143
  77.8 1.4 pad_maximum_fusion
  79.3 0.2 copy.135
  79.5 0.2 copy.134
  79.6 0.3 copy-done.9
  80.0 0.8 reshape.310
  80.7 0.8 reshape.309
  81.5 10.7 %all-to-all-done.2 = bf16[16,64,256]{2,1,0:T(8,128)(2,1)S(1)} async-done(((bf16[16,64,256]{2,1,0:T(8,128)(2,1)}), bf16[16,64,256]{2,1,0:T(8,128)(2,1)S(1)}, u32[]{:S(2)}, u32[]{:S(2)}) %all-to-all-start.2) | async-done | bytes 524320 | tf_op jit(solution)/shard_map/all_to_all | solution.py:25
  92.2 1.3 fusion.68
  93.6 2.0 convolution_convert_fusion
  95.6 0.9 copy.169
  96.4 3.5 %all-to-all-start.3 = ((bf16[16,64,256]{2,1,0:T(8,128)(2,1)}), bf16[16,64,256]{2,1,0:T(8,128)(2,1)S(1)}, u32[]{:S(2)}, u32[]{:S(2)}) async-start(bf16[16,64,256]{2,1,0:T(8,128)(2,1)} %bitcast.119), calls=%async_computation.3 | async-start | bytes 1048576 | tf_op jit(solution)/shard_map/all_to_all | solution.py:19
  99.9 101.3 %all-reduce.2.cloned.1.call-done = bf16[1048576]{0:T(1024)(128)(2,1)} async-done(((bf16[1048576]{0:T(1024)(128)(2,1)}), bf16[1048576]{0:T(1024)(128)(2,1)}) %all-reduce.2.cloned.1.call-update) | async-done | bytes 2097168 | tf_op jit(solution)/shard_map/psum | solution.py:45
  201.2 3.8 %slice_convert_fusion.1 = (f32[524288]{0:T(1024)}, f32[524288]{0:T(1024)}) fusion(bf16[1048576]{0:T(1024)(128)(2,1)} %all-reduce.2.cloned.1.call-done), kind=kLoop, calls=%fused_computation.31 | loop fusion | flops 1048576 | bytes 6291456 | tf_op jit(solution)/shard_map/convert_element_type | solution.py:193
  205.0 2.7 %reshape.311 = f32[16,4,8,1024]{3,2,1,0:T(8,128)} reshape(f32[524288]{0:T(1024)} %get-tuple-element.5) | data formatting | bytes 4194304 | tf_op jit(solution)/shard_map/convert_element_type | solution.py:193
  207.7 2.7 %reshape.312 = f32[16,4,8,1024]{3,2,1,0:T(8,128)} reshape(f32[524288]{0:T(1024)} %get-tuple-element.6) | data formatting | bytes 4194304 | tf_op jit(solution)/shard_map/convert_element_type | solution.py:193
  210.4 3.5 %fusion.21 = bf16[16,4,8,256]{3,2,0,1:T(8,128)(2,1)S(1)} fusion(bf16[4,1024,256]{2,1,0:T(8,128)(2,1)} %param.43, f32[16,4,8,1024]{3,2,1,0:T(8,128)} %reshape.312, f32[16,4,8,1024]{3,2,1,0:T(8,128)} %reshape.311), kind=kOutput, calls=%fused_computation.18 | convolution fusion | flops 271712256 | bytes 6553600 | tf_op jit(solution)/shard_map/secf,efd->secd/dot_general | solution.py:198
  214.0 0.7 copy.171
  214.7 6.7 %all-to-all-start.5 = ((bf16[16,32,256]{2,1,0:T(8,128)(2,1)}), bf16[16,32,256]{2,1,0:T(8,128)(2,1)S(1)}, u32[]{:S(2)}, u32[]{:S(2)}) async-start(bf16[16,32,256]{2,1,0:T(8,128)(2,1)} %bitcast.122), calls=%async_computation.5 | async-start | bytes 524288 | tf_op jit(solution)/shard_map/all_to_all | solution.py:201
  221.4 0.1 select_reduce_fusion
  221.6 5.3 %all-to-all-done.5 = bf16[16,32,256]{2,1,0:T(8,128)(2,1)S(1)} async-done(((bf16[16,32,256]{2,1,0:T(8,128)(2,1)}), bf16[16,32,256]{2,1,0:T(8,128)(2,1)S(1)}, u32[]{:S(2)}, u32[]{:S(2)}) %all-to-all-start.5) | async-done | bytes 262176 | tf_op jit(solution)/shard_map/all_to_all | solution.py:201
  226.9 0.9 fusion.26
  (40 shorter events, 0.9 us)
Async XLA Ops:
  7.2 67.8 %copy-start = (bf16[4,256,1024]{2,1,0:T(8,128)(2,1)S(1)}, bf16[4,256,1024]{2,1,0:T(8,128)(2,1)}, u32[]{:S(2)}) copy-start(bf16[4,256,1024]{2,1,0:T(8,128)(2,1)} %param.42) | copy-start | bytes 6291460
  7.2 6.3 %copy-start.4 = (f32[16,512]{1,0:T(8,128)S(1)}, f32[16,512]{1,0:T(8,128)}, u32[]{:S(2)}) copy-start(f32[16,512]{1,0:T(8,128)} %param.30) | copy-start | bytes 98308
  7.2 6.4 %copy-start.5 = (f32[16,512]{1,0:T(8,128)S(1)}, f32[16,512]{1,0:T(8,128)}, u32[]{:S(2)}) copy-start(f32[16,512]{1,0:T(8,128)} %param.31) | copy-start | bytes 98308
  7.2 6.5 %copy-start.6 = (f32[16,512]{1,0:T(8,128)S(1)}, f32[16,512]{1,0:T(8,128)}, u32[]{:S(2)}) copy-start(f32[16,512]{1,0:T(8,128)} %param.32) | copy-start | bytes 98308
  7.2 6.6 %copy-start.7 = (f32[16,512]{1,0:T(8,128)S(1)}, f32[16,512]{1,0:T(8,128)}, u32[]{:S(2)}) copy-start(f32[16,512]{1,0:T(8,128)} %param.33) | copy-start | bytes 98308
  7.2 6.6 %copy-start.2 = (f32[64,512]{1,0:T(8,128)S(1)}, f32[64,512]{1,0:T(8,128)}, u32[]{:S(2)}) copy-start(f32[64,512]{1,0:T(8,128)} %param.35) | copy-start | bytes 393220
  7.2 6.7 %copy-start.3 = (f32[64,512]{1,0:T(8,128)S(1)}, f32[64,512]{1,0:T(8,128)}, u32[]{:S(2)}) copy-start(f32[64,512]{1,0:T(8,128)} %param.36) | copy-start | bytes 393220
  15.5 12.1 %copy-start.8 = (s32[64,4]{0,1:T(4,128)S(1)}, s32[64,4]{0,1:T(4,128)}, u32[]{:S(2)}) copy-start(s32[64,4]{0,1:T(4,128)} %param.44) | copy-start | bytes 3076
  18.4 26.4 %all-to-all-start = ((bf16[16,64,256]{2,1,0:T(8,128)(2,1)}), bf16[16,64,256]{2,1,0:T(8,128)(2,1)S(1)}, u32[]{:S(2)}, u32[]{:S(2)}) async-start(bf16[16,64,256]{2,1,0:T(8,128)(2,1)} %bitcast.130), calls=%async_computation | async-start | bytes 1048576 | tf_op jit(solution)/shard_map/all_to_all | solution.py:19
  46.4 10.0 %all-to-all-start.1 = ((f32[16,64,1]{1,2,0:T(1,128)}), f32[16,64,1]{1,2,0:T(1,128)S(1)}, u32[]{:S(2)}, u32[]{:S(2)}) async-start(f32[16,64,1]{1,2,0:T(1,128)} %broadcast_in_dim.12), calls=%async_computation.1 | async-start | bytes 16384 | tf_op jit(solution)/shard_map/all_to_all | solution.py:25
  69.6 22.6 %all-to-all-start.2 = ((bf16[16,64,256]{2,1,0:T(8,128)(2,1)}), bf16[16,64,256]{2,1,0:T(8,128)(2,1)S(1)}, u32[]{:S(2)}, u32[]{:S(2)}) async-start(bf16[16,64,256]{2,1,0:T(8,128)(2,1)} %broadcast_in_dim.13), calls=%async_computation.2 | async-start | bytes 1048576 | tf_op jit(solution)/shard_map/all_to_all | solution.py:25
  74.9 126.3 %all-reduce.2.cloned.1.call-start = ((), (), s32[]{:S(2)}) async-start(), calls=%async_computation.6 | async-start | bytes 4194304 | tf_op jit(solution)/shard_map/psum | solution.py:45
  75.4 1.6 copy-start.1
  79.3 0.7 copy-start.9
  96.4 118.3 %all-to-all-start.3 = ((bf16[16,64,256]{2,1,0:T(8,128)(2,1)}), bf16[16,64,256]{2,1,0:T(8,128)(2,1)S(1)}, u32[]{:S(2)}, u32[]{:S(2)}) async-start(bf16[16,64,256]{2,1,0:T(8,128)(2,1)} %bitcast.119), calls=%async_computation.3 | async-start | bytes 1048576 | tf_op jit(solution)/shard_map/all_to_all | solution.py:19
  214.7 12.2 %all-to-all-start.5 = ((bf16[16,32,256]{2,1,0:T(8,128)(2,1)}), bf16[16,32,256]{2,1,0:T(8,128)(2,1)S(1)}, u32[]{:S(2)}, u32[]{:S(2)}) async-start(bf16[16,32,256]{2,1,0:T(8,128)(2,1)} %bitcast.122), calls=%async_computation.5 | async-start | bytes 524288 | tf_op jit(solution)/shard_map/all_to_all | solution.py:201
Sparse Core Ops, SparseCore 0:
  79.4 121.7 all-reduce.1
where the time goes:
time: 239 us; the launch traced here: 235 us
  waiting for transfers between devices  139 us (58%)
  starting transfers between devices  28 us (12%)
  local copies, waits for them, and re-layouts  18 us (8%)
  between operations  14.4 us (6%)
  matrix products  14 us (6%)
  blocking collectives  12.1 us (5%)
  other arithmetic  9.5 us (4%)
    psum x1, waiting for transfers between devices, in_one(): total = lax.psum(line, axis)  101 us
    all_to_all x2, waiting for transfers between devices, sent_to_all(): return lax.all_to_all(copies, axis, split_axis=0, concat_axis=0, tiled=True)  16.4 us
    all_to_all x2, waiting for transfers between devices, sent_and_summed(): lax.all_to_all(parts, axis, split_axis=0, concat_axis=0, tiled=True)  15.7 us
    all_to_all x2, starting transfers between devices, sent_and_summed(): lax.all_to_all(parts, axis, split_axis=0, concat_axis=0, tiled=True)  12.6 us
    all_to_all x1, blocking collectives, local(): lax.all_to_all(outgoing, 'ep', split_axis=0, concat_axis=0, tiled=True)  12.1 us
    all_to_all x2, starting transfers between devices, sent_to_all(): return lax.all_to_all(copies, axis, split_axis=0, concat_axis=0, tiled=True)  8.66 us
    all_to_all x1, starting transfers between devices, local(): lax.all_to_all(expert_terms.reshape(ep_count, expert_dev * capacity, slic...  6.68 us
    convert_element_type x2, local copies, waits for them, and re-layouts, local(): part.astype(jnp.float32)  5.45 us
  transfers between devices with their start and end apart: 6, of which 5 were waited for; matrix products, arithmetic and copies ran while one was open for 11% of the time, Pallas kernels for 0%

commit v1 on v0

v1 whole, which is shorter than its diff:
```python
import functools
import types

import jax
import jax.numpy as jnp
from jax import lax
from jax.experimental import pallas as pl
from jax.experimental.pallas import tpu as pltpu
from jax.sharding import PartitionSpec as P

EPS = 1e-06
ROUTED_SCALE = 2.5
CAP = 8
MESH = pl.DeviceIdType.MESH
F32 = jnp.float32
BF16 = jnp.bfloat16


def mm(a, b):
    return lax.dot_general(a, b, (((1,), (0,)), ((), ())), preferred_element_type=F32)


def mm_nt(a, b):
    return lax.dot_general(a, b, (((1,), (1,)), ((), ())), preferred_element_type=F32)


def iota(shape, dim):
    return lax.broadcasted_iota(jnp.int32, shape, dim)


def silu(v):
    return v / (1.0 + jnp.exp(-v))


def layer(d, *refs):
    n = types.SimpleNamespace(**dict(zip(d.names, refs)))
    ep, tp = lax.axis_index("ep"), lax.axis_index("tp")
    z, c = lax.div(tp, 2), lax.rem(tp, 2)
    oc = 1 - c
    HS, FD, CD, CR, K = d.HS, d.FD, d.CD, d.CR, d.K

    open_scope = []

    def mark(name=None):
        if open_scope:
            open_scope.pop().__exit__(None, None, None)
        if name:
            open_scope.append(jax.named_scope(name))
            open_scope[-1].__enter__()

    mark("greet")
    barrier = pltpu.get_barrier_semaphore()

    def greet_tp(i, carry):
        pl.semaphore_signal(barrier, inc=1, device_id=(ep, lax.rem(tp + i, d.TP)), device_id_type=MESH)
        return carry

    def greet_ep(i, carry):
        for cc in range(2):
            pl.semaphore_signal(
                barrier, inc=1, device_id=(lax.rem(ep + i, d.EP), z * 2 + cc), device_id_type=MESH
            )
        return carry

    lax.fori_loop(1, d.TP, greet_tp, 0)
    lax.fori_loop(1, d.EP, greet_ep, 0)

    mark("loads")
    loads = {}

    def load(name, src, dst):
        loads[name] = pltpu.make_async_copy(src, dst, n.lsem.at[len(loads)])
        loads[name].start()

    load("tok", n.tokens, n.tok)
    load("ng", n.norm_gain, n.ng)
    load("win", n.w_in, n.win)
    load("ls", n.log_step, n.ls)
    load("dec", n.decay_rate, n.dec)
    load("frq", n.frequency, n.frq)
    load("ir", n.input_real, n.ir)
    load("ii", n.input_imag, n.ii)
    load("rt", n.routing, n.rt)
    load("rw", n.route_weight, n.rw)
    load("sr", n.state_real, n.sr)
    load("si", n.state_imag, n.si)
    load("our", n.readout_real, n.our)
    load("oui", n.readout_imag, n.oui)
    load("sk", n.skip_gain, n.sk)
    load("wout", n.w_out, n.wout)
    load("fg", n.ffn_gain, n.fg)
    load("eg", n.expert_gate.at[pl.ds(c * 2, 2)], n.eg.at[c])
    load("eu", n.expert_up.at[pl.ds(c * 2, 2)], n.eu.at[c])
    load("sg", n.shared_gate, n.sgu.at[pl.ds(c * d.FSD, d.FSD)])
    load("su", n.shared_up, n.sgu.at[pl.ds((2 + c) * d.FSD, d.FSD)])
    load("sd", n.shared_down, n.sd.at[pl.ds(c * d.FSD, d.FSD)])
    load("ed", n.expert_down.at[pl.ds(c * 2, 2)], n.ed.at[c])

    mark("slots")
    loads["rt"].wait()
    loads["rw"].wait()
    which = iota((d.E, d.S), 0)
    raw = n.rw[...]
    share = ROUTED_SCALE * raw / jnp.sum(raw, axis=0, keepdims=True)
    member = jnp.zeros((d.E, d.S), F32)
    weight = jnp.zeros((d.E, d.S), F32)
    for k in range(d.KT):
        hit = n.rt[k : k + 1, :] == which
        member = member + jnp.where(hit, 1.0, 0.0)
        weight = weight + jnp.where(hit, share[k : k + 1, :], 0.0)
    before = jnp.where(iota((d.S, d.S), 0) < iota((d.S, d.S), 1), 1.0, 0.0).astype(BF16)
    rank = mm(member.astype(BF16), before)
    wide = (d.E, CAP, d.S)
    slot = jnp.where(
        (jnp.broadcast_to(rank[:, None, :], wide) == iota(wide, 1).astype(F32))
        & (jnp.broadcast_to(member[:, None, :], wide) > 0.5),
        1.0,
        0.0,
    )
    n.place[...] = slot.reshape(d.E * CAP, d.S).astype(BF16)
    shares = (slot * jnp.broadcast_to(weight[:, None, :], wide)).reshape(d.E * CAP, d.S)
    n.comb[...] = shares.T

    mark("poles")
    for name in ("ls", "dec", "frq", "ir", "ii"):
        loads[name].wait()
    lane = iota((1, d.NS), 1)
    step = jnp.zeros((1, d.NS), F32)
    steps = jnp.exp(n.ls[...])
    for g in range(d.G):
        step = jnp.where(lax.div(lane, d.ST) == g, steps[:, g : g + 1], step)
    decay, omega = n.dec[...], n.frq[...]
    mag = jnp.exp(-decay * step)
    angle = omega * step
    pole_re, pole_im = mag * jnp.cos(angle), mag * jnp.sin(angle)
    norm = decay * decay + omega * omega
    diff = pole_re - 1.0
    lift_re = (-decay * diff + omega * pole_im) / norm
    lift_im = (-decay * pole_im - omega * diff) / norm
    in_re, in_im = n.ir[...], n.ii[...]
    own_group = lax.div(iota((d.CH, d.NS), 0), d.CHAN) == lax.div(iota((d.CH, d.NS), 1), d.ST)

    def spread(x):
        return jnp.where(own_group, jnp.concatenate([x] * d.G, axis=0), 0.0)

    map_re = spread(in_re * lift_re - in_im * lift_im)
    map_im = spread(in_re * lift_im + in_im * lift_re)
    hi_re, hi_im = map_re.astype(BF16), map_im.astype(BF16)
    lo_re = (map_re - hi_re.astype(F32)).astype(BF16)
    lo_im = (map_im - hi_im.astype(F32)).astype(BF16)

    mark("wait_tok")
    for name in ("tok", "ng", "win"):
        loads[name].wait()

    mark("project")
    def project(i, carry):
        squares, total = carry
        cols = pl.ds(pl.multiple_of(i * d.KB, d.KB), d.KB)
        x = n.tok[:, cols].astype(F32)
        squares = squares + jnp.sum(x * x, axis=1, keepdims=True)
        total = total + mm((x * n.ng[:, cols]).astype(BF16), n.win[cols, :])
        return squares, total

    squares, total = lax.fori_loop(
        0, d.D // d.KB, project, (jnp.zeros((d.S, 1), F32), jnp.zeros((d.S, d.CH), F32))
    )
    drive = (total * lax.rsqrt(squares / d.D + EPS)).astype(BF16)

    mark("state")
    for name in ("sr", "si", "our", "oui", "sk"):
        loads[name].wait()
    old_re, old_im = n.sr[...], n.si[...]
    new_re = pole_re * old_re - pole_im * old_im + (mm(drive, hi_re) + mm(drive, lo_re))
    new_im = pole_re * old_im + pole_im * old_re + (mm(drive, hi_im) + mm(drive, lo_im))
    n.nr[...] = new_re
    n.ni[...] = new_im
    save_re = pltpu.make_async_copy(n.nr, n.out_re, n.osem.at[0])
    save_im = pltpu.make_async_copy(n.ni, n.out_im, n.osem.at[1])
    save_re.start()
    save_im.start()
    read = mm_nt(new_re.astype(BF16), spread(n.our[...]).astype(BF16)) - mm_nt(
        new_im.astype(BF16), spread(n.oui[...]).astype(BF16)
    )
    read = read + n.sk[...] * drive.astype(F32)
    act = jax.nn.gelu(read).astype(BF16)
    first = c == 0

    mark("mix_parts")
    loads["wout"].wait()
    for zz in range(d.Z):
        part = mm(act, n.wout[:, zz * CD : (zz + 1) * CD]).astype(BF16)
        for h in range(2):
            n.mix[zz, h] = part[:, h * FD : (h + 1) * FD]

    mark("barrier")
    pl.semaphore_wait(barrier, d.TP - 1 + 2 * (d.EP - 1))

    partner = (ep, z * 2 + oc)

    def chip_at(j):
        away = ((j + 1) // 2) * (1 - 2 * (j % 2))
        return lax.rem(z + K + away + d.Z, d.Z)

    def pair_copy(j):
        zz = chip_at(j)
        if j < d.Z - 1:
            src, dst = n.mix.at[zz, :, pl.ds(oc * HS, HS)], n.pair.at[j]
        else:
            src, dst = n.mix.at[z, oc], n.pair_own
        return pltpu.make_async_remote_copy(
            src, dst, n.gsem.at[0], n.psem.at[j], device_id=partner, device_id_type=MESH
        )

    mark("pair")
    n.mix_recv[pl.ds(z * 2, 2)] = jnp.zeros((2, HS, FD), BF16)
    for j in range(d.Z):
        pair_copy(j).start()
    swaps = {}

    def swap(name, src, dst):
        i = len(swaps)
        swaps[name] = pltpu.make_async_remote_copy(
            src, dst, n.wssem.at[i], n.wrsem.at[i], device_id=partner, device_id_type=MESH
        )
        swaps[name].start()


    def tp_sends(src_at, recv, ssem, rsem):
        def go(zz, cc):
            pltpu.make_async_remote_copy(
                src_at(zz, cc), recv.at[tp], ssem, rsem, device_id=(ep, zz * 2 + cc), device_id_type=MESH
            ).start()

        for j in range(d.Z - 1):
            zz = chip_at(j)
            go(zz, 0)
            go(zz, 1)
        go(z, oc)

    def landed(ref, count, sem):
        view = ref.at[pl.ds(0, count)]
        pltpu.make_async_copy(view, view, sem).wait()

    def total_of(recv):
        halves = []
        for h in range(2):
            acc = recv[h].astype(F32)
            for zz in range(1, d.Z):
                acc = acc + recv[zz * 2 + h].astype(F32)
            halves.append(acc)
        return jnp.concatenate(halves, axis=0)

    hops = {(0, 0): K, (0, 1): K - 1, (1, 0): K - 1, (1, 1): K}
    flows = ((0, 0), (1, 1), (0, 1), (1, 0))
    ahead = (lax.rem(z + 1, d.Z), lax.rem(z + d.Z - 1, d.Z))

    def number(way, h, t):
        return (way * 2 + h) * K + t

    def owner_of(way, away):
        return lax.rem(z + (away if way == 0 else d.Z - away), d.Z)

    def small_ring(value, send, recv, last, ssem, rsem, lsem):
        def copy(way, h, t):
            i = number(way, h, t)
            if t == hops[way, h] - 1:
                dst, sem, core = last.at[way * 2 + c], lsem.at[way * 2 + c], h
            else:
                dst, sem, core = recv.at[i], rsem.at[i], c
            return pltpu.make_async_remote_copy(
                send.at[i], dst, ssem, sem, device_id=(ep, ahead[way] * 2 + core), device_id_type=MESH
            )

        def step(way, h, t):
            i = number(way, h, t)
            total = value(way, hops[way, h] - t, h)
            if t > 0:
                copy(way, h, t - 1).wait_recv()
                total = total + recv[i - 1].astype(F32)
            send[i] = total.astype(BF16)
            copy(way, h, t).start()

        def arrived(way, core):
            pltpu.make_async_remote_copy(
                send.at[0],
                last.at[way * 2 + core],
                ssem,
                lsem.at[way * 2 + core],
                device_id=(ep, ahead[way] * 2 + core),
                device_id_type=MESH,
            ).wait_recv()
            return last[way * 2 + core].astype(F32)

        return step, arrived

    mark("mix_send")
    for j in range(d.Z - 1):
        zz = chip_at(j)
        pair_copy(j).wait_recv()
        for h in range(2):
            both = n.mix[zz, h, pl.ds(c * HS, HS)].astype(F32) + n.pair[j, h].astype(F32)
            n.mix_send[j * 2 + h] = both.astype(BF16)
            pltpu.make_async_remote_copy(
                n.mix_send.at[j * 2 + h],
                n.mix_recv.at[tp],
                n.gsem.at[1],
                n.gsem.at[13],
                device_id=(ep, zz * 2 + h),
                device_id_type=MESH,
            ).start()
    mark("mix_wait")
    loads["fg"].wait()
    mine = pl.ds(pl.multiple_of(tp * FD, FD), FD)
    own_tok = n.tok[:, mine].astype(F32)
    own_gain = n.fg[:, mine]
    pair_copy(d.Z - 1).wait_recv()
    mixer = n.mix[z, c].astype(F32) + n.pair_own[...].astype(F32)
    landed(n.mix_recv, d.TP - 2, n.gsem.at[13])
    mixer = mixer + total_of(n.mix_recv)

    swap("eg", n.expert_gate.at[pl.ds(oc * 2, 2)], n.eg.at[c])
    swap("eu", n.expert_up.at[pl.ds(oc * 2, 2)], n.eu.at[c])
    swap("sg", n.shared_gate, n.sgu.at[pl.ds(c * d.FSD, d.FSD)])
    swap("su", n.shared_up, n.sgu.at[pl.ds((2 + c) * d.FSD, d.FSD)])
    mark("dispatch")
    resid = (own_tok + mixer).astype(BF16)
    n.resid[...] = resid
    resid_f = resid.astype(F32)
    rows = (resid_f * own_gain).astype(BF16)

    n.disp_send[...] = mm(n.place[...], rows).astype(BF16).reshape(2 * d.EP, 2 * CAP, FD)

    def dispatch(ee, cc):
        pltpu.make_async_remote_copy(
            n.disp_send.at[ee * 2 + cc],
            n.xin.at[c * d.EP + ep],
            n.gsem.at[2],
            n.gsem.at[3],
            device_id=(ee, z * 2 + cc),
            device_id_type=MESH,
        ).start()

    def dispatch_body(i, carry):
        ee = lax.rem(ep + i, d.EP)
        dispatch(ee, 0)
        dispatch(ee, 1)
        return carry

    lax.fori_loop(1, d.EP, dispatch_body, 0)
    dispatch(ep, oc)
    n.xin[c * d.EP + ep] = n.disp_send[ep * 2 + c]

    mark("squares_rows")
    per_row = jnp.sum(resid_f * resid_f, axis=1, keepdims=True)
    turned = jnp.where(iota((d.S, 128), 0) == iota((d.S, 128), 1), per_row, 0.0)
    n.ss_send[...] = jnp.sum(turned, axis=0, keepdims=True)
    n.ss_recv[tp] = n.ss_send[...]
    tp_sends(lambda zz, cc: n.ss_send, n.ss_recv, n.gsem.at[4], n.gsem.at[5])
    n.rows_send[...] = rows.reshape(2, HS, FD)
    n.rows_recv[tp] = n.rows_send[c]
    tp_sends(lambda zz, cc: n.rows_send.at[cc], n.rows_recv, n.gsem.at[6], n.gsem.at[7])

    swap("sd", n.shared_down, n.sd.at[pl.ds(c * d.FSD, d.FSD)])
    swap("ed", n.expert_down.at[pl.ds(oc * 2, 2)], n.ed.at[c])

    mark("ss_wait")
    landed(n.ss_recv, d.TP - 1, n.gsem.at[5])
    square = n.ss_recv[0]
    for i in range(1, d.TP):
        square = square + n.ss_recv[i]
    factor = lax.rsqrt(square / d.D + EPS)
    row8 = iota((8, 128), 0)
    piece1 = factor.astype(BF16).astype(F32)
    piece2 = (factor - piece1).astype(BF16).astype(F32)
    piece3 = factor - piece1 - piece2
    pieces = jnp.where(row8 == 0, piece1, jnp.where(row8 == 1, piece2, jnp.where(row8 == 2, piece3, 0.0)))
    spread_fac = mm_nt(pieces.astype(BF16)[:, : d.S], n.place[...])
    n.fac_send[...] = jnp.sum(spread_fac, axis=0, keepdims=True)
    n.fac_recv[ep] = n.fac_send[...]

    def fac_body(i, carry):
        pltpu.make_async_remote_copy(
            n.fac_send,
            n.fac_recv.at[ep],
            n.gsem.at[8],
            n.gsem.at[9],
            device_id=(lax.rem(ep + i, d.EP), tp),
            device_id_type=MESH,
        ).start()
        return carry

    lax.fori_loop(1, d.EP, fac_body, 0)

    mark("factors")
    for name in ("eg", "eu"):
        loads[name].wait()
        swaps[name].wait_recv()
    mark("disp_wait")
    landed(n.xin, 2 * d.EP - 1, n.gsem.at[3])
    mark("gate_up")
    half_row = lax.div(lax.rem(iota((d.EP * 2 * CAP, FD), 0), 2 * CAP), CAP)
    for f in range(2):
        x = n.xin[f * d.EP : (f + 1) * d.EP].reshape(d.EP * 2 * CAP, FD).astype(F32)
        for e in range(2):
            n.xm[f, e] = jnp.where(half_row == e, x, 0.0).astype(BF16)

    per_half = d.FH // d.NB

    def gate_up(i, carry):
        cols = pl.ds(pl.multiple_of(i * d.NB, d.NB), d.NB)
        h = lax.div(i, per_half)
        at = lax.rem(i, per_half) * d.NB
        for w, base in ((n.eg, 0), (n.eu, d.FH)):
            acc = jnp.zeros((d.EP * 2 * CAP, d.NB), F32)
            for f in range(2):
                for e in range(2):
                    acc = acc + mm(n.xm[f, e], w[f, e, :, cols])
            n.part[h, :, pl.ds(pl.multiple_of(base + at, d.NB), d.NB)] = acc.astype(BF16)
        return carry

    lax.fori_loop(0, d.FE // d.NB, gate_up, 0)

    mark("ring0")
    def owned(o):
        return pl.ds(pl.multiple_of(o * CR, CR), CR)

    def ring_copy(way, h, t):
        i = number(way, h, t)
        away = hops[way, h] - t
        owner = lax.rem(z + (away if way == 0 else d.Z - away), d.Z)
        if t == 0:
            src = n.part.at[h, owned(owner)]
        else:
            src = n.rs_send.at[i]
        return owner, pltpu.make_async_remote_copy(
            src, n.rs_recv.at[i], n.rsssem, n.rsrsem.at[i], device_id=(ep, ahead[way] * 2 + c), device_id_type=MESH
        )

    def ring_step(way, h, t):
        owner, copy = ring_copy(way, h, t)
        if t > 0:
            ring_copy(way, h, t - 1)[1].wait_recv()
            i = number(way, h, t)
            n.rs_send[i] = (n.rs_recv[i - 1].astype(F32) + n.part[h, owned(owner)].astype(F32)).astype(BF16)
        copy.start()

    for way, h in flows:
        ring_step(way, h, 0)
    for way, h in flows:
        ring_step(way, h, 1)

    mark("rows_wait")
    for name in ("sg", "su"):
        loads[name].wait()
        swaps[name].wait_recv()
    landed(n.rows_recv, d.TP - 1, n.gsem.at[7])
    mark("shared")
    all_rows = jnp.concatenate([n.rows_recv[i] for i in range(d.TP)], axis=1)
    both = mm_nt(all_rows, n.sgu[...])
    own_fac = jnp.sum(
        jnp.where(iota((HS, 128), 1) == iota((HS, 128), 0) + c * HS, factor, 0.0), axis=1, keepdims=True
    )
    shared_inner = (silu(both[:, : 2 * d.FSD] * own_fac) * (both[:, 2 * d.FSD :] * own_fac)).astype(BF16)

    mark("shared_down")
    for name in ("sd",):
        loads[name].wait()
        swaps[name].wait_recv()
    for zz in range(d.Z):
        part = mm(shared_inner, n.sd[:, zz * CD : (zz + 1) * CD]).astype(BF16)
        for h in range(2):
            n.sh[zz, h] = part[:, h * FD : (h + 1) * FD]
    sh_pair = pltpu.make_async_remote_copy(
        n.sh.at[z, oc], n.sh_pair, n.assem, n.arsem, device_id=partner, device_id_type=MESH
    )
    sh_pair.start()

    def sh_value(way, away, h):
        return n.sh[owner_of(way, away), h].astype(F32)

    sh_step, sh_arrived = small_ring(
        sh_value, n.sh_send, n.sh_recv, n.sh_last, n.gsem.at[12], n.shsem, n.shlsem
    )

    mark("ring")
    for t in range(2, K):
        for way, h in flows:
            if t < hops[way, h]:
                ring_step(way, h, t)

    mark("sh0")
    for way, h in flows:
        sh_step(way, h, 0)
    mark("fac_wait")
    landed(n.fac_recv, d.EP - 1, n.gsem.at[9])
    slots = 2 * CAP
    at_slot = iota((slots, d.E * CAP), 0) + ep * (2 * slots) + c * slots
    here = iota((slots, d.E * CAP), 1) == at_slot
    column = jnp.concatenate(
        [
            jnp.sum(jnp.where(here, n.fac_recv[z * d.BPO + b], 0.0), axis=1, keepdims=True)
            for b in range(d.BPO)
        ],
        axis=0,
    )
    mark("ring_last")
    own = owned(z)
    for h in range(2):
        acc = n.part[h, own].astype(F32)
        for way in range(2):
            t = hops[way, h] - 1
            ring_copy(way, h, t)[1].wait_recv()
            acc = acc + n.rs_recv[number(way, h, t)].astype(F32)
        acc = acc * column
        n.inner[h, z] = (silu(acc[:, : d.FH]) * acc[:, d.FH :]).astype(BF16)

    mark("pass0")
    def pass_copy(way, h, t):
        i = number(way, h, t)
        owner = lax.rem(z + (d.Z - t if way == 0 else t), d.Z)
        return pltpu.make_async_remote_copy(
            n.inner.at[h, owner],
            n.inner.at[h, owner],
            n.agssem,
            n.agrsem.at[i],
            device_id=(ep, ahead[way] * 2 + c),
            device_id_type=MESH,
        )

    def arrival(way, h, t):
        i = number(way, h, t)
        owner = lax.rem(z + (d.Z - t - 1 if way == 0 else t + 1), d.Z)
        pltpu.make_async_remote_copy(
            n.inner.at[h, owner],
            n.inner.at[h, owner],
            n.agssem,
            n.agrsem.at[i],
            device_id=(ep, ahead[way] * 2 + c),
            device_id_type=MESH,
        ).wait_recv()

    def down(*owners):
        rows = CR * len(owners)
        odd = lax.div(lax.rem(iota((rows, d.FH), 0), 2 * CAP), CAP)
        accs = [jnp.zeros((rows, FD), F32), jnp.zeros((rows, FD), F32)]
        for h in range(2):
            x = jnp.concatenate([n.inner[h, o].astype(F32) for o in owners], axis=0)
            for e in range(2):
                xe = jnp.where(odd == e, x, 0.0).astype(BF16)
                for f in range(2):
                    accs[f] = accs[f] + mm(xe, n.ed[f, e, h * d.FH : (h + 1) * d.FH, :])
        blocks = [o * d.BPO + b for o in owners for b in range(d.BPO)]
        for i, ee in enumerate(blocks):
            for f in range(2):
                n.ret_send[ee * 2 + f] = accs[f][i * 2 * CAP : (i + 1) * 2 * CAP].astype(BF16)
        for ee in blocks:
            for f in range(2):
                give_back(ee, f)

    def give_back(ee, f):
        is_me = (ee == ep) & (c == f)

        @pl.when(is_me)
        def _():
            n.ret_recv[ep * 2 + c] = n.ret_send[ee * 2 + f]

        @pl.when(jnp.logical_not(is_me))
        def _():
            pltpu.make_async_remote_copy(
                n.ret_send.at[ee * 2 + f],
                n.ret_recv.at[ep * 2 + c],
                n.gsem.at[10],
                n.gsem.at[11],
                device_id=(ee, z * 2 + f),
                device_id_type=MESH,
            ).start()

    for way, h in flows:
        pass_copy(way, h, 0).start()

    mark("sh1")
    for way, h in flows:
        sh_step(way, h, 1)
    mark("down0")
    loads["ed"].wait()
    swaps["ed"].wait_recv()
    down(z)
    for t in range(1, K):
        mark("pass")
        for way, h in flows:
            arrival(way, h, t - 1)
            if t < hops[way, h]:
                pass_copy(way, h, t).start()
        mark("sh_step")
        for way, h in flows:
            if t + 1 < hops[way, h]:
                sh_step(way, h, t + 1)
        mark("down")
        down(lax.rem(z + d.Z - t, d.Z), lax.rem(z + t, d.Z))
    mark("pass_last")
    arrival(0, 0, K - 1)
    arrival(1, 1, K - 1)
    mark("down_last")
    down(lax.rem(z + K, d.Z))
    mark("sh_wait")
    comb = n.comb[...]
    comb_hi = comb.astype(BF16)
    comb_lo = (comb - comb_hi.astype(F32)).astype(BF16)
    base = n.resid[...].astype(F32)
    sh_pair.wait_recv()
    halves = [sh_arrived(0, core) + sh_arrived(1, core) for core in range(2)]
    mine_sh, other_sh = n.sh[z, c].astype(F32), n.sh_pair[...].astype(F32)
    base = base + jnp.concatenate(
        [halves[0] + jnp.where(first, mine_sh, other_sh), halves[1] + jnp.where(first, other_sh, mine_sh)],
        axis=0,
    )
    mark("ret_wait")
    landed(n.ret_recv, 2 * d.EP - 1, n.gsem.at[11])
    mark("join")
    back = n.ret_recv[...].reshape(d.E * CAP, FD)
    n.fin[...] = (base + mm(comb_hi, back) + mm(comb_lo, back)).astype(BF16)
    save = pltpu.make_async_copy(n.fin, n.out_mixed, n.osem.at[2])
    save.start()

    mark("drain")
    sh_pair.wait_send()
    for copy in swaps.values():
        copy.wait_send()
    landed(n.pair, d.Z, n.gsem.at[0])
    landed(n.mix_send, d.TP - 2, n.gsem.at[1])
    landed(n.disp_send, 2 * d.EP - 1, n.gsem.at[2])
    landed(n.ss_recv, d.TP - 1, n.gsem.at[4])
    landed(n.rows_recv, d.TP - 1, n.gsem.at[6])
    landed(n.fac_recv, d.EP - 1, n.gsem.at[8])
    landed(n.ret_send, 2 * d.EP - 1, n.gsem.at[10])
    landed(n.sh_send, 4 * K - 2, n.gsem.at[12])
    landed(n.rs_recv, 4 * K - 2, n.rsssem)
    view = n.agdummy.at[pl.ds(0, 4 * K - 2)]
    pltpu.make_async_copy(view, view, n.agssem).wait()
    save_re.wait()
    save_im.wait()
    save.wait()
    mark()


def hand_out(*refs):
    srcs, dsts, bufs, sem = refs[:3], refs[3:6], refs[6:9], refs[9]
    ins = [pltpu.make_async_copy(s, b, sem.at[i]) for i, (s, b) in enumerate(zip(srcs, bufs))]
    outs = [pltpu.make_async_copy(b, t, sem.at[3 + i]) for i, (b, t) in enumerate(zip(bufs, dsts))]
    for copy in ins:
        copy.start()
    for copy, after in zip(ins, outs):
        copy.wait()
        after.start()
    for copy in outs:
        copy.wait()


ARGS = (
    "tokens",
    "norm_gain",
    "ffn_gain",
    "w_in",
    "decay_rate",
    "frequency",
    "log_step",
    "input_real",
    "input_imag",
    "readout_real",
    "readout_imag",
    "skip_gain",
    "state_real",
    "state_imag",
    "w_out",
    "shared_gate",
    "shared_up",
    "shared_down",
    "expert_gate",
    "expert_up",
    "expert_down",
    "routing",
    "route_weight",
)


def local(d, *args):
    a = dict(zip(ARGS, args))
    for name in ("norm_gain", "ffn_gain", "decay_rate", "frequency", "log_step", "skip_gain"):
        a[name] = a[name].reshape(1, -1)
    for name in ("shared_gate", "shared_up", "routing", "route_weight"):
        a[name] = a[name].T
    d = types.SimpleNamespace(**vars(d))
    d.S, d.D = a["tokens"].shape
    d.HS = d.S // 2
    d.FD = d.D // d.TP
    d.CD = 2 * d.FD
    d.CH = a["w_in"].shape[1]
    d.NS = a["decay_rate"].shape[1]
    d.G = a["log_step"].shape[1]
    d.ST = d.NS // d.G
    d.CHAN = d.CH // d.G
    d.FE = a["expert_gate"].shape[2]
    d.FH = d.FE // 2
    d.NB = min(256, d.FH)
    d.FSD = a["shared_down"].shape[0]
    d.KT = a["routing"].shape[0]
    d.E = d.EP * 4
    d.BPO = d.EP // d.Z
    d.CR = d.BPO * 2 * CAP
    d.K = d.Z // 2
    d.KB = min(512, d.D)
    v = pltpu.VMEM
    dma = pltpu.SemaphoreType.DMA
    ring = 4 * d.K
    scratch = dict(
        tok=v((d.S, d.D), BF16),
        ng=v((1, d.D), F32),
        fg=v((1, d.D), F32),
        win=v((d.D, d.CH), BF16),
        ls=v((1, d.G), F32),
        dec=v((1, d.NS), F32),
        frq=v((1, d.NS), F32),
        ir=v((d.CHAN, d.NS), F32),
        ii=v((d.CHAN, d.NS), F32),
        our=v((d.CHAN, d.NS), F32),
        oui=v((d.CHAN, d.NS), F32),
        sk=v((1, d.CH), F32),
        sr=v((d.S, d.NS), F32),
        si=v((d.S, d.NS), F32),
        nr=v((d.S, d.NS), F32),
        ni=v((d.S, d.NS), F32),
        rt=v((d.KT, d.S), jnp.int32),
        rw=v((d.KT, d.S), F32),
        wout=v((d.CH, d.D), BF16),
        sgu=v((4 * d.FSD, d.D), BF16),
        sd=v((2 * d.FSD, d.D), BF16),
        eg=v((2, 2, d.FD, d.FE), BF16),
        eu=v((2, 2, d.FD, d.FE), BF16),
        ed=v((2, 2, d.FE, d.FD), BF16),
        place=v((d.E * CAP, d.S), BF16),
        comb=v((d.S, d.E * CAP), F32),
        mix=v((d.Z, 2, d.S, d.FD), BF16),
        pair=v((d.Z, 2, d.HS, d.FD), BF16),
        pair_own=v((d.S, d.FD), BF16),
        mix_send=v((d.TP - 2, d.HS, d.FD), BF16),
        mix_recv=v((d.TP, d.HS, d.FD), BF16),
        resid=v((d.S, d.FD), BF16),
        disp_send=v((2 * d.EP, 2 * CAP, d.FD), BF16),
        xin=v((2 * d.EP, 2 * CAP, d.FD), BF16),
        xm=v((2, 2, d.EP * 2 * CAP, d.FD), BF16),
        ss_send=v((1, 128), F32),
        ss_recv=v((d.TP, 1, 128), F32),
        rows_send=v((2, d.HS, d.FD), BF16),
        rows_recv=v((d.TP, d.HS, d.FD), BF16),
        fac_send=v((1, d.E * CAP), F32),
        fac_recv=v((d.EP, 1, d.E * CAP), F32),
        part=v((2, d.EP * 2 * CAP, d.FE), BF16),
        rs_send=v((ring, d.CR, d.FE), BF16),
        rs_recv=v((ring, d.CR, d.FE), BF16),
        inner=v((2, d.Z, d.CR, d.FH), BF16),
        agdummy=v((ring, d.CR, d.FH), BF16),
        ret_send=v((2 * d.EP, 2 * CAP, d.FD), BF16),
        ret_recv=v((2 * d.EP, 2 * CAP, d.FD), BF16),
        sh=v((d.Z, 2, d.HS, d.FD), BF16),
        sh_pair=v((d.HS, d.FD), BF16),
        sh_send=v((ring, d.HS, d.FD), BF16),
        sh_recv=v((ring, d.HS, d.FD), BF16),
        sh_last=v((4, d.HS, d.FD), BF16),
        fin=v((d.S, d.FD), BF16),
        lsem=dma((23,)),
        osem=dma((3,)),
        wssem=dma((6,)),
        wrsem=dma((6,)),
        psem=dma((d.Z,)),
        shsem=dma((ring,)),
        shlsem=dma((4,)),
        assem=dma,
        arsem=dma,
        gsem=dma((14,)),
        rsssem=dma,
        rsrsem=dma((ring,)),
        agssem=dma,
        agrsem=dma((ring,)),
    )
    d.names = tuple(ARGS) + ("out_mixed", "out_re", "out_im") + tuple(scratch)
    anywhere = pl.BlockSpec(memory_space=pl.ANY)
    results = pl.pallas_call(
        functools.partial(layer, d),
        out_shape=(
            jax.ShapeDtypeStruct((d.S, d.FD), BF16),
            jax.ShapeDtypeStruct((d.S, d.NS), F32),
            jax.ShapeDtypeStruct((d.S, d.NS), F32),
        ),
        in_specs=[anywhere] * len(ARGS),
        out_specs=(anywhere,) * 3,
        scratch_shapes=list(scratch.values()),
        compiler_params=pltpu.CompilerParams(
            collective_id=0, has_side_effects=True, vmem_limit_bytes=67043328
        ),
        name="layer",
    )(*[a[name] for name in ARGS])
    return pl.pallas_call(
        hand_out,
        out_shape=tuple(jax.ShapeDtypeStruct(r.shape, r.dtype) for r in results),
        in_specs=[anywhere] * 3,
        out_specs=(anywhere,) * 3,
        scratch_shapes=[v(r.shape, r.dtype) for r in results] + [dma((6,))],
        compiler_params=pltpu.CompilerParams(vmem_limit_bytes=67043328),
        name="hand_out",
    )(*results)


def solution(mesh):
    d = types.SimpleNamespace(EP=mesh.shape["ep"], TP=mesh.shape["tp"], Z=mesh.shape["tp"] // 2)
    placed = (
        P("ep", None),
        P(),
        P(),
        P(None, "tp"),
        P("tp"),
        P("tp"),
        P("tp"),
        P(None, "tp"),
        P(None, "tp"),
        P(None, "tp"),
        P(None, "tp"),
        P("tp"),
        P("ep", "tp"),
        P("ep", "tp"),
        P("tp", None),
        P(None, "tp"),
        P(None, "tp"),
        P("tp", None),
        P("ep", "tp", None),
        P("ep", "tp", None),
        P("ep", None, "tp"),
        P("ep", None),
        P("ep", None),
    )
    return jax.shard_map(
        functools.partial(local, d),
        mesh=mesh,
        in_specs=placed,
        out_specs=(P("ep", "tp"), P("ep", "tp"), P("ep", "tp")),
        check_vma=False,
    )
```

time: 239 us -> 65.3 us (0.27); the launches traced: 235 us -> 65.2 us
  waiting for transfers between devices: 139 us -> 0 us
  Pallas kernels: 0 us -> 64.6 us
  starting transfers between devices: 28 us -> 0 us
  local copies, waits for them, and re-layouts: 18 us -> 0 us
  matrix products: 14 us -> 0 us
  between operations: 14.4 us -> 0.65 us
  blocking collectives: 12.1 us -> 0 us
  other arithmetic: 9.5 us -> 0 us
    psum x1 -> x0, waiting for transfers between devices: 101 us -> none  [in_one(): total = lax.psum(line, axis)]
    pallas_call x0 -> x2, Pallas kernels: none -> 64.6 us  [the longest x1 62.9 us: local(): pl.pallas_call(functools.partial(layer, d), out_shape=(jax.ShapeDtypeStru...]
    all_to_all x5 -> x0, waiting for transfers between devices: 37.4 us -> none  [the longest x2 16.4 us: sent_to_all(): return lax.all_to_all(copies, axis, split_axis=0, concat_axis=0, tiled=True)]
    all_to_all x5 -> x0, starting transfers between devices: 28 us -> none  [the longest x2 12.6 us: sent_and_summed(): lax.all_to_all(parts, axis, split_axis=0, concat_axis=0, tiled=True)]
    dot_general x13 -> x0, matrix products: 14 us -> none  [the longest x1 3.54 us: local(): jnp.einsum('secf,efd->secd', inner_rows, expert_down, preferred_element_t...]
    all_to_all x1 -> x0, blocking collectives: 12.1 us -> none  [local(): lax.all_to_all(outgoing, 'ep', split_axis=0, concat_axis=0, tiled=True)]
    convert_element_type x6 -> x0, local copies, waits for them, and re-layouts: 6.46 us -> none  [the longest x2 5.45 us: local(): part.astype(jnp.float32)]
    reshape x12 -> x0, local copies, waits for them, and re-layouts: 4.56 us -> none  [the longest x2 1.7 us: split_up(): parts = x.reshape(*dims[:dim], peers, dims[dim] // peers, *dims[dim + 1:])]
  transfers between devices with their start and end apart: 6 -> 0, of which waited for: 5 -> 0; matrix products, arithmetic and copies ran while one was open for 11% -> 0% of each run, Pallas kernels for 0% -> 0%
where the time goes in v1:
time: 65.3 us; the launch traced here: 65.2 us
  Pallas kernels  64.6 us (99%)
    pallas_call x1, Pallas kernels, local(): pl.pallas_call(functools.partial(layer, d), out_shape=(jax.ShapeDtypeStru...  62.9 us
    pallas_call x1, Pallas kernels, local(): pl.pallas_call(hand_out, out_shape=tuple((jax.ShapeDtypeStruct(r.shape, r...  1.69 us

profile of v1, /device:TPU:17, one launch (start us, length us, event | category | flops | bytes accessed | tf_op | source)
XLA Modules:
  0.0 65.2 jit_solution(1399245435591533457)
XLA Ops:
  0.6 62.9 %layer.1 = (bf16[64,256]{1,0:T(8,128)(2,1)}, f32[64,512]{1,0:T(8,128)}, f32[64,512]{1,0:T(8,128)}) custom-call(bf16[64,4096]{1,0:T(8,128)(2,1)} %refs_0_.1, f32[1,4096]{1,0:T(1,128)} %bitcast.12, f32[1,4096]{1,0:T(1,128)} %bitcast.13, bf16[4096,128]{1,0:T(8,128)(2,1)} %refs_3_.1, f32[1,512]{1,0:T(1,128)} %bitcast.14, f32[1,512]{1,0:T(1,128)} %bitcast.15, ...), custom_call_target="tpu_custom_call" | custom-call | tf_op jit(solution)/shard_map/layer/pallas_call | solution.py:788
  63.5 1.7 %hand_out.1 = (bf16[64,256]{1,0:T(8,128)(2,1)}, f32[64,512]{1,0:T(8,128)}, f32[64,512]{1,0:T(8,128)}) custom-call(bf16[64,256]{1,0:T(8,128)(2,1)} %get-tuple-element.6.refs_0_, f32[64,512]{1,0:T(8,128)} %get-tuple-element.7.refs_1_, f32[64,512]{1,0:T(8,128)} %get-tuple-element.8.refs_2_), custom_call_target="tpu_custom_call" | custom-call | tf_op jit(solution)/shard_map/hand_out/pallas_call | solution.py:803
